TPU v7x, 512 devices: a whole 4x8x8 slice. The times are simulated.
512 devices in a mesh: ep: 128 (over z, y, core), tp: 4 (over x).
Axes of the slice: x: 4, y: 8, z: 8, core: 2. Of those that a mesh axis runs over, the one named last changes fastest.
Arguments:
- residual_in: bfloat16 [2560, 1024], P('ep', 'tp'), may hold values from -64 to 64
- queries: bfloat16 [2560, 512], P(('ep', 'tp')), may hold values from -6 to 6
- cache_keys: bfloat16 [2560, 1024, 128], P(('ep', 'tp')), may hold values from -6 to 6
- cache_values: bfloat16 [2560, 1024, 128], P(('ep', 'tp')), may hold values from -24 to 24
- lengths: int32 [2560], P(('ep', 'tp')), may hold values from 256 to 1024
- stick_offset: float32 [8], replicated, may hold values from 0.5 to 6
- out_weight: bfloat16 [512, 1024], P(None, 'tp'), may hold values from -0.25 to 0.25
- norm1_gain: float32 [1024], P('tp'), may hold values from 0.3 to 3.1
- norm1_bias: float32 [1024], P('tp'), may hold values from -1.5 to 1.5
- routes: int32 [2560, 6], P('ep'), may hold values from 0 to 127, all different within a row; in each aligned block of 20 rows (0 to 19, 20 to 39, ...) at most 2 rows name the same one
- route_weights: float32 [2560, 6], P('ep'), may hold values from 0.1 to 0.8
- expert_gate: bfloat16 [128, 1024, 512], P('ep', None, 'tp'), may hold values from -0.1875 to 0.1875
- expert_up: bfloat16 [128, 1024, 512], P('ep', None, 'tp'), may hold values from -0.1875 to 0.1875
- expert_down: bfloat16 [128, 512, 1024], P('ep', 'tp'), may hold values from -0.25 to 0.25
- shared_gate: bfloat16 [1024, 512], P(None, 'tp'), may hold values from -0.1875 to 0.1875
- shared_up: bfloat16 [1024, 512], P(None, 'tp'), may hold values from -0.1875 to 0.1875
- shared_down: bfloat16 [512, 1024], P('tp'), may hold values from -0.25 to 0.25
- norm2_gain: float32 [1024], P('tp'), may hold values from 0.1 to 1.9
- norm2_bias: float32 [1024], P('tp'), may hold values from -1.5 to 1.5
Outputs:
- layer_out: bfloat16 [2560, 1024], P('ep', 'tp')
Inputs may be any that keep to these rules, and one draw needn't show every extreme that they name: `routes`: each row names 6 different experts; among the rows of one index of ep no expert is named more than 2 times.
All inputs are finite; a program needn't handle non-finite values.
Results may differ from a plain program's by a relative error of at most 0.0095.
Values may be sent and summed in bfloat16 or wider, within the bound.
No kernel may reach another device: no remote copies, remote signals or barrier semaphores. Data moves between devices by JAX's collectives and lax.ppermute only.
A program may use at most 64 MiB of HBM per device.

v0:
```python
import jax
import jax.numpy as jnp
from jax import lax
from jax.sharding import PartitionSpec as P

H = 8
HD = 64
KVH = 2
CACHE = 1024
TOPK = 6
RESIDUAL_SCALE = 2.0**0.25
EPSILON = 1e-05


def joined_along(blocks, dim):
    blocks = jnp.moveaxis(blocks, 0, dim)
    shape = blocks.shape
    return blocks.reshape(*shape[:dim], shape[dim] * shape[dim + 1], *shape[dim + 2 :])


def from_everyone(value, axis):
    copies = jnp.broadcast_to(value, (lax.axis_size(axis), *value.shape))
    return lax.all_to_all(copies, axis, split_axis=0, concat_axis=0, tiled=True)


def gathered_copies(value, axis, dim):
    return joined_along(from_everyone(value, axis), dim)


def rows_first(arrays, axis, dims):
    turned = [jnp.moveaxis(a, dim, 0) for a, dim in zip(arrays, dims)]
    both = jnp.concatenate([t.reshape(len(t), -1) for t in turned], axis=1)
    out, at, done = (lax.all_gather(both, axis, axis=0, tiled=True), 0, [])
    for t, dim in zip(turned, dims):
        piece = out[:, at : at + t[0].size].reshape(-1, *t.shape[1:])
        done.append(jnp.moveaxis(piece, 0, dim))
        at += t[0].size
    return tuple(done)


def cut_along(value, dim, devices):
    before, after = (value.shape[:dim], value.shape[dim + 1 :])
    return jnp.moveaxis(value.reshape(*before, devices, -1, *after), dim, 0)


def sent_and_summed(value, axis, dim):
    blocks = cut_along(value, dim, lax.axis_size(axis))
    arrived = lax.all_to_all(blocks, axis, split_axis=0, concat_axis=0, tiled=True)
    return arrived.astype(jnp.float32).sum(axis=0)


def over_copies(value, axis):
    everything = from_everyone(value, axis)
    return jnp.sum(everything, axis=0)


def packed_total(arrays, axis):
    ends = [0]
    for a in arrays:
        ends.append(ends[-1] + a.size)
    running = over_copies(jnp.concatenate([a.ravel() for a in arrays]), axis)
    return tuple((running[b:e].reshape(a.shape) for a, b, e in zip(arrays, ends, ends[1:])))


def normalize(totals, squares, entries, values, scales, shifts):
    centre = totals / entries
    spread = squares / entries - centre * centre
    return (values - centre) * lax.rsqrt(spread + EPSILON) * scales + shifts


def stick_read(queries, keys_block, values_block, lengths, offsets):
    seq_count = queries.shape[0]
    grouped = H // KVH
    query_heads = queries.reshape(seq_count, KVH, grouped, HD)
    key_heads = keys_block.reshape(seq_count, CACHE, KVH, HD)
    value_heads = values_block.reshape(seq_count, CACHE, KVH, HD)
    scores = jnp.einsum(
        "sgjd,slgd->sgjl", query_heads, key_heads, preferred_element_type=jnp.float32
    )
    scores = scores * HD ** (-0.5) - offsets.reshape(1, KVH, grouped, 1)
    live_mask = (jnp.arange(CACHE)[None, :] < lengths[:, None])[:, None, None, :]
    keep_log = jnp.where(live_mask, jax.nn.log_sigmoid(-scores), 0.0)
    after_log = lax.cumsum(keep_log, axis=3, reverse=True) - keep_log
    weights = jnp.where(live_mask, jnp.exp(jax.nn.log_sigmoid(scores) + after_log), 0.0)
    weights = weights.astype(jnp.bfloat16)
    mixed = jnp.einsum("sgjl,slgd->sgjd", weights, value_heads, preferred_element_type=jnp.float32)
    return mixed.reshape(seq_count, H * HD).astype(jnp.bfloat16)


def body(
    residual_in,
    queries,
    cache_keys,
    cache_values,
    lengths,
    stick_offset,
    out_weight,
    norm1_gain,
    norm1_bias,
    routes,
    route_weights,
    expert_gate,
    expert_up,
    expert_down,
    shared_gate,
    shared_up,
    shared_down,
    norm2_gain,
    norm2_bias,
):
    mixed = stick_read(queries, cache_keys, cache_values, lengths, stick_offset)
    attended = jnp.dot(
        gathered_copies(mixed, "tp", 0), out_weight, preferred_element_type=jnp.float32
    )
    before = RESIDUAL_SCALE * residual_in.astype(jnp.float32) + attended
    group_rows, columns = residual_in.shape
    full_width = columns * lax.axis_size("tp")
    widened, scales, shifts = rows_first((before, norm1_gain, norm1_bias), "tp", (1, 0, 0))
    whole = normalize(
        jnp.sum(widened, axis=1, keepdims=True),
        jnp.sum(widened * widened, axis=1, keepdims=True),
        full_width,
        widened,
        scales,
        shifts,
    ).astype(jnp.bfloat16)
    normed = lax.dynamic_slice_in_dim(whole, lax.axis_index("tp") * columns, columns, 1)
    experts = lax.axis_size("ep")
    capacity = min(group_rows, 2 * ((group_rows * TOPK + experts - 1) // experts))
    slots_all = experts * capacity
    chosen = routes.reshape(-1)
    order_ids = jnp.arange(chosen.shape[0])
    matches = (chosen[:, None] == chosen[None, :]) & (order_ids[None, :] < order_ids[:, None])
    targets = chosen * capacity + jnp.sum(matches.astype(jnp.int32), axis=1)
    picks = (targets[:, None] == jnp.arange(slots_all)[None, :]).astype(jnp.float32)
    picks = picks.reshape(group_rows, TOPK, slots_all)
    dispatch = jnp.sum(picks, axis=1).astype(jnp.bfloat16)
    combine = jnp.sum(picks * route_weights[:, :, None], axis=1)
    parcel = jnp.einsum("sr,sd->rd", dispatch, whole, preferred_element_type=jnp.float32)
    parcel = parcel.astype(jnp.bfloat16).reshape(experts, capacity, full_width)
    arrived = lax.all_to_all(parcel, "ep", split_axis=0, concat_axis=0, tiled=True)
    gate_part = jnp.einsum(
        "ecd,df->ecf", arrived, expert_gate[0], preferred_element_type=jnp.float32
    )
    up_part = jnp.einsum("ecd,df->ecf", arrived, expert_up[0], preferred_element_type=jnp.float32)
    hidden = (jax.nn.silu(gate_part) * up_part).astype(jnp.bfloat16)
    partial_value = jnp.einsum(
        "ecf,fd->ecd", hidden, expert_down[0], preferred_element_type=jnp.float32
    )
    summed = sent_and_summed(partial_value.astype(jnp.bfloat16), "tp", 2).astype(jnp.bfloat16)
    returned = lax.all_to_all(summed, "ep", split_axis=0, concat_axis=0, tiled=True)
    routed = jnp.dot(
        combine,
        returned.reshape(slots_all, columns).astype(jnp.float32),
        precision=lax.Precision.HIGHEST,
    )
    shared_hidden = (
        jax.nn.silu(jnp.dot(whole, shared_gate, preferred_element_type=jnp.float32))
        * jnp.dot(whole, shared_up, preferred_element_type=jnp.float32)
    ).astype(jnp.bfloat16)
    shared_term = jnp.dot(shared_hidden, shared_down, preferred_element_type=jnp.float32)
    shared = sent_and_summed(shared_term.astype(jnp.bfloat16), "tp", 1)
    after = RESIDUAL_SCALE * normed.astype(jnp.float32) + routed + shared
    final_totals, final_squares = packed_total(
        (jnp.sum(after, axis=1), jnp.sum(after * after, axis=1)), "tp"
    )
    return normalize(
        final_totals[:, None], final_squares[:, None], full_width, after, norm2_gain, norm2_bias
    ).astype(jnp.bfloat16)


def solution(mesh):
    in_specs = (
        P("ep", "tp"),
        P(("ep", "tp"), None),
        P(("ep", "tp"), None, None),
        P(("ep", "tp"), None, None),
        P(("ep", "tp")),
        P(),
        P(None, "tp"),
        P("tp"),
        P("tp"),
        P("ep", None),
        P("ep", None),
        P("ep", None, "tp"),
        P("ep", None, "tp"),
        P("ep", "tp", None),
        P(None, "tp"),
        P(None, "tp"),
        P("tp", None),
        P("tp"),
        P("tp"),
    )
    out_specs = P("ep", "tp")
    return jax.shard_map(body, mesh=mesh, in_specs=in_specs, out_specs=out_specs, check_vma=False)
```

profile of v0, /device:TPU:1, one launch (start us, length us, event | category | flops | bytes accessed | tf_op | source)
XLA Modules:
  0.0 168.4 jit_solution(15376619532127802602)
XLA Ops:
  0.0 0.8 iota_compare_fusion.2
  0.8 1.6 copy.87
  2.4 0.1 reshape.116
  2.5 0.1 sub.42
  2.6 0.4 fusion.19
  3.1 49.5 %reduce-window.6 = f32[5,2,4,8,128]{4,3,2,1,0:T(8,128)S(1)} reduce-window(f32[5,2,4,8,128]{4,3,2,1,0:T(8,128)S(1)} %reshape.118, f32[]{:T(128)} %constant.30.clone.1), window={size=1x1x1x1x128 pad=0_0x0_0x0_0x0_0x0_127}, to_apply=%region_0.1 | reduce-window | flops 5201920 | bytes 327684 | tf_op jit(solution)/shard_map/reduce-window
  52.6 0.1 slice_reduce_fusion
  52.7 1.8 %reduce-window.9 = f32[5,2,4,9]{3,2,1,0:T(4,128)S(1)} reduce-window(f32[5,2,4,8]{3,2,1,0:T(4,128)S(1)} %slice_reduce_fusion, f32[]{:T(128)} %constant.30.clone.1), window={size=1x1x1x8 pad=0_0x0_0x0_0x0_8}, to_apply=%region_1.2 | reduce-window | flops 2520 | bytes 2724 | tf_op jit(solution)/shard_map/reduce-window.1
  54.5 0.1 slice.29
  54.6 0.1 broadcast_add_fusion
  54.8 0.6 copy.88
  55.5 0.6 convolution_convert_fusion.3
  56.1 0.1 convert_element_type.53
  56.2 0.6 broadcast_in_dim.19
  56.8 4.8 %all-to-all-start = ((bf16[4,5,512]{2,1,0:T(8,128)(2,1)}), bf16[4,5,512]{2,1,0:T(8,128)(2,1)S(1)}, u32[]{:S(2)}, u32[]{:S(2)}) async-start(bf16[4,5,512]{2,1,0:T(8,128)(2,1)} %broadcast_in_dim.19), calls=%async_computation | async-start | bytes 65536 | tf_op jit(solution)/shard_map/all_to_all | solution.py:23
  61.6 0.1 copy.89
  61.7 0.1 eq.29
  61.8 0.2 convert_reduce_fusion.2
  62.0 0.1 reduce_sum.98
  62.1 0.1 copy.90
  62.2 0.1 convert_reduce_fusion
  62.3 3.6 %all-to-all-done = bf16[4,5,512]{2,1,0:T(8,128)(2,1)S(1)} async-done(((bf16[4,5,512]{2,1,0:T(8,128)(2,1)}), bf16[4,5,512]{2,1,0:T(8,128)(2,1)S(1)}, u32[]{:S(2)}, u32[]{:S(2)}) %all-to-all-start) | async-done | bytes 20512 | tf_op jit(solution)/shard_map/all_to_all | solution.py:23
  66.0 0.2 fusion.3
  66.2 9.0 %all_gather.3 = f32[1024,22]{0,1:T(8,128)S(1)} all-gather(f32[256,22]{0,1:T(8,128)S(1)} %pad_maximum_fusion), channel_id=1, replica_groups=mesh['ep'=128,'tp'=4] {'tp'}, dimensions={0}, use_global_device_ids=true | all-gather | bytes 112640 | tf_op jit(solution)/shard_map/all_gather | solution.py:33
  75.2 0.1 slice_reduce_fusion.1
  75.4 0.1 add_convert_fusion
  75.5 0.3 convolution_convert_fusion.1
  75.8 0.2 reshape.124
  76.0 42.3 %all_to_all.31 = bf16[128,2,1024]{2,1,0:T(2,128)(2,1)S(1)} all-to-all(bf16[128,2,1024]{2,1,0:T(2,128)(2,1)S(1)} %reshape.124), channel_id=1, replica_groups=mesh['ep'=128,'tp'=4] {'ep'}, dimensions={0} | all-to-all | bytes 1048576 | tf_op jit(solution)/shard_map/all_to_all | solution.py:141
  118.3 0.3 fusion.7
  118.6 0.5 convolution_convert_fusion
  119.2 0.8 copy.107
  120.0 3.5 %all-to-all-start.2 = ((bf16[4,128,2,256]{3,1,2,0:T(8,128)(2,1)}), bf16[4,128,2,256]{3,1,2,0:T(8,128)(2,1)S(1)}, u32[]{:S(2)}, u32[]{:S(2)}) async-start(bf16[4,128,2,256]{3,1,2,0:T(8,128)(2,1)} %bitcast.48), calls=%async_computation.2 | async-start | bytes 1048576 | tf_op jit(solution)/shard_map/all_to_all | solution.py:48
  123.5 0.2 fusion.43
  123.7 0.3 convolution_convert_fusion.2
  124.0 0.6 copy.108
  124.6 8.6 %all-to-all-done.2 = bf16[4,128,2,256]{3,1,2,0:T(8,128)(2,1)S(1)} async-done(((bf16[4,128,2,256]{3,1,2,0:T(8,128)(2,1)}), bf16[4,128,2,256]{3,1,2,0:T(8,128)(2,1)S(1)}, u32[]{:S(2)}, u32[]{:S(2)}) %all-to-all-start.2) | async-done | bytes 524320 | tf_op jit(solution)/shard_map/all_to_all | solution.py:48
  133.3 3.3 %all-to-all-start.4 = ((bf16[4,20,256]{2,1,0:T(8,128)(2,1)}), bf16[4,20,256]{2,1,0:T(8,128)(2,1)S(1)}, u32[]{:S(2)}, u32[]{:S(2)}) async-start(bf16[4,20,256]{2,1,0:T(8,128)(2,1)} %bitcast.49), calls=%async_computation.4 | async-start | bytes 98304 | tf_op jit(solution)/shard_map/all_to_all | solution.py:48
  136.5 0.1 reduce_sum.101
  136.6 0.8 copy.95
  137.4 3.5 %all-to-all-done.4 = bf16[4,20,256]{2,1,0:T(8,128)(2,1)S(1)} async-done(((bf16[4,20,256]{2,1,0:T(8,128)(2,1)}), bf16[4,20,256]{2,1,0:T(8,128)(2,1)S(1)}, u32[]{:S(2)}, u32[]{:S(2)}) %all-to-all-start.4) | async-done | bytes 40992 | tf_op jit(solution)/shard_map/all_to_all | solution.py:48
  140.9 6.9 %all-to-all-start.3 = ((bf16[128,2,256]{2,1,0:T(2,128)(2,1)}), bf16[128,2,256]{2,1,0:T(2,128)(2,1)S(1)}, u32[]{:S(2)}, u32[]{:S(2)}) async-start(bf16[128,2,256]{2,1,0:T(2,128)(2,1)} %copy.95), calls=%async_computation.3 | async-start | bytes 262144 | tf_op jit(solution)/shard_map/all_to_all | solution.py:151
  147.9 12.8 %all-to-all-done.3 = bf16[128,2,256]{2,1,0:T(2,128)(2,1)S(1)} async-done(((bf16[128,2,256]{2,1,0:T(2,128)(2,1)}), bf16[128,2,256]{2,1,0:T(2,128)(2,1)S(1)}, u32[]{:S(2)}, u32[]{:S(2)}) %all-to-all-start.3) | async-done | bytes 131104 | tf_op jit(solution)/shard_map/all_to_all | solution.py:151
  160.7 0.3 fusion.41
  161.0 0.1 pad_maximum_fusion.1
  161.1 6.5 %all_to_all.32 = f32[4,1,40]{2,1,0:T(1,128)S(1)} all-to-all(f32[4,1,40]{2,1,0:T(1,128)S(1)} %broadcast_in_dim.20), channel_id=1, replica_groups=mesh['ep'=128,'tp'=4] {'tp'}, dimensions={0} | all-to-all | bytes 1280 | tf_op jit(solution)/shard_map/all_to_all | solution.py:23
  167.6 0.1 slice_multiply_fusion
  167.7 0.7 add_convert_fusion.1
  (46 shorter events, 0.4 us)
Async XLA Ops:
  0.0 118.6 %copy-start = (bf16[1,128,1024]{2,1,0:T(8,128)(2,1)S(1)}, bf16[1,128,1024]{2,1,0:T(8,128)(2,1)}, u32[]{:S(2)}) copy-start(bf16[1,128,1024]{2,1,0:T(8,128)(2,1)} %param.32) | copy-start | bytes 786436
  0.8 1.6 copy-start.8
  0.8 1.7 %copy-start.16 = (f32[8]{0:T(128)S(1)}, f32[8]{0:T(128)}, u32[]{:S(2)}) copy-start(f32[8]{0:T(128)} %param.24) | copy-start | bytes 100
  2.6 52.2 %copy-start.1 = (bf16[5,1024,128]{2,1,0:T(8,128)(2,1)S(1)}, bf16[5,1024,128]{2,1,0:T(8,128)(2,1)}, u32[]{:S(2)}) copy-start(bf16[5,1024,128]{2,1,0:T(8,128)(2,1)} %param.22) | copy-start | bytes 3932164
  55.4 6.2 %copy-start.6 = (s32[20,6]{0,1:T(8,128)S(1)}, s32[20,6]{0,1:T(8,128)}, u32[]{:S(2)}) copy-start(s32[20,6]{0,1:T(8,128)} %param.28) | copy-start | bytes 1444
  55.4 6.8 %copy-start.9 = (f32[20,6]{0,1:T(8,128)S(1)}, f32[20,6]{0,1:T(8,128)}, u32[]{:S(2)}) copy-start(f32[20,6]{0,1:T(8,128)} %param.29) | copy-start | bytes 1444
  55.4 10.5 %copy-start.2 = (bf16[512,256]{1,0:T(8,128)(2,1)S(1)}, bf16[512,256]{1,0:T(8,128)(2,1)}, u32[]{:S(2)}) copy-start(bf16[512,256]{1,0:T(8,128)(2,1)} %param.25) | copy-start | bytes 786436
  55.5 10.5 %copy-start.7 = (bf16[20,256]{1,0:T(8,128)(2,1)S(1)}, bf16[20,256]{1,0:T(8,128)(2,1)}, u32[]{:S(2)}) copy-start(bf16[20,256]{1,0:T(8,128)(2,1)} %param.19) | copy-start | bytes 30724
  55.5 10.7 %copy-start.10 = (f32[256]{0:T(256)S(1)}, f32[256]{0:T(256)}, u32[]{:S(2)}) copy-start(f32[256]{0:T(256)} %param.27) | copy-start | bytes 3076
  55.5 10.7 %copy-start.11 = (f32[256]{0:T(256)S(1)}, f32[256]{0:T(256)}, u32[]{:S(2)}) copy-start(f32[256]{0:T(256)} %param.26) | copy-start | bytes 3076
  56.8 9.1 %all-to-all-start = ((bf16[4,5,512]{2,1,0:T(8,128)(2,1)}), bf16[4,5,512]{2,1,0:T(8,128)(2,1)S(1)}, u32[]{:S(2)}, u32[]{:S(2)}) async-start(bf16[4,5,512]{2,1,0:T(8,128)(2,1)} %broadcast_in_dim.19), calls=%async_computation | async-start | bytes 65536 | tf_op jit(solution)/shard_map/all_to_all | solution.py:23
  75.5 42.8 %copy-start.14 = (bf16[1,1024,128]{2,1,0:T(8,128)(2,1)S(1)}, bf16[1,1024,128]{2,1,0:T(8,128)(2,1)}, u32[]{:S(2)}) copy-start(bf16[1,1024,128]{2,1,0:T(8,128)(2,1)} %param.30) | copy-start | bytes 786436
  75.8 42.8 %copy-start.15 = (bf16[1,1024,128]{2,1,0:T(8,128)(2,1)S(1)}, bf16[1,1024,128]{2,1,0:T(8,128)(2,1)}, u32[]{:S(2)}) copy-start(bf16[1,1024,128]{2,1,0:T(8,128)(2,1)} %param.31) | copy-start | bytes 786436
  119.1 4.3 %copy-start.3 = (bf16[1024,128]{1,0:T(8,128)(2,1)S(1)}, bf16[1024,128]{1,0:T(8,128)(2,1)}, u32[]{:S(2)}) copy-start(bf16[1024,128]{1,0:T(8,128)(2,1)} %param.33) | copy-start | bytes 786436
  119.1 4.5 %copy-start.4 = (bf16[128,1024]{1,0:T(8,128)(2,1)S(1)}, bf16[128,1024]{1,0:T(8,128)(2,1)}, u32[]{:S(2)}) copy-start(bf16[128,1024]{1,0:T(8,128)(2,1)} %param.35) | copy-start | bytes 786436
  119.2 4.5 %copy-start.5 = (bf16[1024,128]{1,0:T(8,128)(2,1)S(1)}, bf16[1024,128]{1,0:T(8,128)(2,1)}, u32[]{:S(2)}) copy-start(bf16[1024,128]{1,0:T(8,128)(2,1)} %param.34) | copy-start | bytes 786436
  120.0 13.3 %all-to-all-start.2 = ((bf16[4,128,2,256]{3,1,2,0:T(8,128)(2,1)}), bf16[4,128,2,256]{3,1,2,0:T(8,128)(2,1)S(1)}, u32[]{:S(2)}, u32[]{:S(2)}) async-start(bf16[4,128,2,256]{3,1,2,0:T(8,128)(2,1)} %bitcast.48), calls=%async_computation.2 | async-start | bytes 1048576 | tf_op jit(solution)/shard_map/all_to_all | solution.py:48
  123.7 44.0 %copy-start.12 = (f32[256]{0:T(256)S(1)}, f32[256]{0:T(256)}, u32[]{:S(2)}) copy-start(f32[256]{0:T(256)} %param.37) | copy-start | bytes 3076
  123.7 44.0 %copy-start.13 = (f32[256]{0:T(256)S(1)}, f32[256]{0:T(256)}, u32[]{:S(2)}) copy-start(f32[256]{0:T(256)} %param.36) | copy-start | bytes 3076
  133.3 7.6 %all-to-all-start.4 = ((bf16[4,20,256]{2,1,0:T(8,128)(2,1)}), bf16[4,20,256]{2,1,0:T(8,128)(2,1)S(1)}, u32[]{:S(2)}, u32[]{:S(2)}) async-start(bf16[4,20,256]{2,1,0:T(8,128)(2,1)} %bitcast.49), calls=%async_computation.4 | async-start | bytes 98304 | tf_op jit(solution)/shard_map/all_to_all | solution.py:48
  140.9 19.8 %all-to-all-start.3 = ((bf16[128,2,256]{2,1,0:T(2,128)(2,1)}), bf16[128,2,256]{2,1,0:T(2,128)(2,1)S(1)}, u32[]{:S(2)}, u32[]{:S(2)}) async-start(bf16[128,2,256]{2,1,0:T(2,128)(2,1)} %copy.95), calls=%async_computation.3 | async-start | bytes 262144 | tf_op jit(solution)/shard_map/all_to_all | solution.py:151
where the time goes:
time: 169 us; the launch traced here: 168 us
  blocking collectives  57.8 us (34%)
  other arithmetic  53.7 us (32%)
  waiting for transfers between devices  28.5 us (17%)
  starting transfers between devices  18.5 us (11%)
  local copies, waits for them, and re-layouts  6.46 us (4%)
  matrix products  3.03 us (2%)
    another operation x3, other arithmetic  51.4 us
    all_to_all x1, blocking collectives, body(): lax.all_to_all(parcel, 'ep', split_axis=0, concat_axis=0, tiled=True)  42.3 us
    all_to_all x1, waiting for transfers between devices, body(): lax.all_to_all(summed, 'ep', split_axis=0, concat_axis=0, tiled=True)  12.8 us
    all_to_all x2, waiting for transfers between devices, sent_and_summed(): lax.all_to_all(blocks, axis, split_axis=0, concat_axis=0, tiled=True)  12.1 us
    all_gather x1, blocking collectives, rows_first(): out, at, done = (lax.all_gather(both, axis, axis=0, tiled=True), 0, [])  9.04 us
    all_to_all x1, starting transfers between devices, body(): lax.all_to_all(summed, 'ep', split_axis=0, concat_axis=0, tiled=True)  6.93 us
    all_to_all x2, starting transfers between devices, sent_and_summed(): lax.all_to_all(blocks, axis, split_axis=0, concat_axis=0, tiled=True)  6.74 us
    all_to_all x1, blocking collectives, from_everyone(): return lax.all_to_all(copies, axis, split_axis=0, concat_axis=0, tiled=True)  6.47 us
  transfers between devices with their start and end apart: 4, of which 4 were waited for; matrix products, arithmetic and copies ran while one was open for 2% of the time, Pallas kernels for 0%

commit v1 on v0

--- a/solution.py
+++ b/solution.py
@@ -30,7 +30,13 @@
 def rows_first(arrays, axis, dims):
     turned = [jnp.moveaxis(a, dim, 0) for a, dim in zip(arrays, dims)]
     both = jnp.concatenate([t.reshape(len(t), -1) for t in turned], axis=1)
-    out, at, done = (lax.all_gather(both, axis, axis=0, tiled=True), 0, [])
+    out, at, done = (
+        jnp.concatenate(
+            lax.all_to_all(jnp.stack([both] * lax.axis_size(axis)), axis, 0, 0), axis=0
+        ),
+        0,
+        [],
+    )
     for t, dim in zip(turned, dims):
         piece = out[:, at : at + t[0].size].reshape(-1, *t.shape[1:])
         done.append(jnp.moveaxis(piece, 0, dim))

time: 169 us -> 167 us (0.988)
  blocking collectives: 57.8 us -> 47 us
  waiting for transfers between devices: 28.5 us -> 33.1 us
  starting transfers between devices: 18.5 us -> 21.8 us
    all_gather x1 -> x0, blocking collectives: 9.04 us -> none  [rows_first(): out, at, done = (lax.all_gather(both, axis, axis=0, tiled=True), 0, [])]
    all_to_all x0 -> x1, waiting for transfers between devices: none -> 4.49 us  [rows_first(): lax.all_to_all(jnp.stack([both] * lax.axis_size(axis)), axis, 0, 0)]
    all_to_all x0 -> x1, starting transfers between devices: none -> 3.3 us  [rows_first(): lax.all_to_all(jnp.stack([both] * lax.axis_size(axis)), axis, 0, 0)]
    all_to_all x1, blocking collectives: 42.3 us -> 40.5 us  [body(): lax.all_to_all(parcel, 'ep', split_axis=0, concat_axis=0, tiled=True)]
  transfers between devices with their start and end apart: 4 -> 5, of which waited for: 4 -> 5; matrix products, arithmetic and copies ran while one was open for 2% -> 2% of each run, Pallas kernels for 0% -> 0%
where the time goes in v1:
time: 167 us; the launch traced here: 166 us
  other arithmetic  53.7 us (32%)
  blocking collectives  47 us (28%)
  waiting for transfers between devices  33.1 us (20%)
  starting transfers between devices  21.8 us (13%)
  local copies, waits for them, and re-layouts  7.16 us (4%)
  matrix products  3.03 us (2%)
    another operation x3, other arithmetic  51.4 us
    all_to_all x1, blocking collectives, body(): lax.all_to_all(parcel, 'ep', split_axis=0, concat_axis=0, tiled=True)  40.5 us
    all_to_all x1, waiting for transfers between devices, body(): lax.all_to_all(summed, 'ep', split_axis=0, concat_axis=0, tiled=True)  12.8 us
    all_to_all x2, waiting for transfers between devices, sent_and_summed(): lax.all_to_all(blocks, axis, split_axis=0, concat_axis=0, tiled=True)  12.1 us
    all_to_all x1, starting transfers between devices, body(): lax.all_to_all(summed, 'ep', split_axis=0, concat_axis=0, tiled=True)  6.93 us
    all_to_all x2, starting transfers between devices, sent_and_summed(): lax.all_to_all(blocks, axis, split_axis=0, concat_axis=0, tiled=True)  6.74 us
    all_to_all x1, blocking collectives, from_everyone(): return lax.all_to_all(copies, axis, split_axis=0, concat_axis=0, tiled=True)  6.47 us
    all_to_all x1, starting transfers between devices, from_everyone(): return lax.all_to_all(copies, axis, split_axis=0, concat_axis=0, tiled=True)  4.83 us
  transfers between devices with their start and end apart: 5, of which 5 were waited for; matrix products, arithmetic and copies ran while one was open for 2% of the time, Pallas kernels for 0%

profile of v1, /device:TPU:1, one launch (start us, length us, event | category | flops | bytes accessed | tf_op | source)
XLA Modules:
  0.0 166.2 jit_solution(1837122258802336481)
XLA Ops:
  0.0 0.8 iota_compare_fusion.2
  0.8 1.6 copy.92
  2.4 0.1 reshape.121
  2.5 0.1 sub.42
  2.6 0.4 fusion.19
  3.1 49.5 %reduce-window.6 = f32[5,2,4,8,128]{4,3,2,1,0:T(8,128)S(1)} reduce-window(f32[5,2,4,8,128]{4,3,2,1,0:T(8,128)S(1)} %reshape.123, f32[]{:T(128)} %constant.30.clone.1), window={size=1x1x1x1x128 pad=0_0x0_0x0_0x0_0x0_127}, to_apply=%region_0.1 | reduce-window | flops 5201920 | bytes 327684 | tf_op jit(solution)/shard_map/reduce-window
  52.6 0.1 slice_reduce_fusion
  52.7 1.8 %reduce-window.9 = f32[5,2,4,9]{3,2,1,0:T(4,128)S(1)} reduce-window(f32[5,2,4,8]{3,2,1,0:T(4,128)S(1)} %slice_reduce_fusion, f32[]{:T(128)} %constant.30.clone.1), window={size=1x1x1x8 pad=0_0x0_0x0_0x0_8}, to_apply=%region_1.2 | reduce-window | flops 2520 | bytes 2724 | tf_op jit(solution)/shard_map/reduce-window.1
  54.6 0.1 broadcast_add_fusion
  54.8 0.6 copy.93
  55.5 0.6 convolution_convert_fusion.3
  56.1 0.1 convert_element_type.53
  56.2 0.6 broadcast_in_dim.19
  56.8 4.8 %all-to-all-start = ((bf16[4,5,512]{2,1,0:T(8,128)(2,1)}), bf16[4,5,512]{2,1,0:T(8,128)(2,1)S(1)}, u32[]{:S(2)}, u32[]{:S(2)}) async-start(bf16[4,5,512]{2,1,0:T(8,128)(2,1)} %broadcast_in_dim.19), calls=%async_computation | async-start | bytes 65536 | tf_op jit(solution)/shard_map/all_to_all | solution.py:23
  61.6 0.1 copy.95
  61.7 0.1 eq.29
  61.8 0.2 convert_reduce_fusion.2
  62.0 0.1 reduce_sum.98
  62.1 0.1 copy.96
  62.2 3.7 %all-to-all-done = bf16[4,5,512]{2,1,0:T(8,128)(2,1)S(1)} async-done(((bf16[4,5,512]{2,1,0:T(8,128)(2,1)}), bf16[4,5,512]{2,1,0:T(8,128)(2,1)S(1)}, u32[]{:S(2)}, u32[]{:S(2)}) %all-to-all-start) | async-done | bytes 20512 | tf_op jit(solution)/shard_map/all_to_all | solution.py:23
  66.0 0.2 fusion.3
  66.2 0.6 stack.2
  66.8 3.3 %all-to-all-start.1 = ((f32[4,256,22]{1,2,0:T(8,128)}), f32[4,256,22]{1,2,0:T(8,128)S(1)}, u32[]{:S(2)}, u32[]{:S(2)}) async-start(f32[4,256,22]{1,2,0:T(8,128)} %stack.2), calls=%async_computation.1 | async-start | bytes 196608 | tf_op jit(solution)/shard_map/all_to_all | solution.py:35
  70.1 0.1 convert_reduce_fusion
  70.2 4.5 %all-to-all-done.1 = f32[4,256,22]{1,2,0:T(8,128)S(1)} async-done(((f32[4,256,22]{1,2,0:T(8,128)}), f32[4,256,22]{1,2,0:T(8,128)S(1)}, u32[]{:S(2)}, u32[]{:S(2)}) %all-to-all-start.1) | async-done | bytes 90144 | tf_op jit(solution)/shard_map/all_to_all | solution.py:35
  74.8 0.1 slice_reduce_fusion.1
  75.0 0.1 add_convert_fusion
  75.1 0.3 convolution_convert_fusion.1
  75.4 0.2 reshape.130
  75.6 40.5 %all_to_all.36 = bf16[128,2,1024]{2,1,0:T(2,128)(2,1)S(1)} all-to-all(bf16[128,2,1024]{2,1,0:T(2,128)(2,1)S(1)} %reshape.130), channel_id=1, replica_groups=mesh['ep'=128,'tp'=4] {'ep'}, dimensions={0} | all-to-all | bytes 1048576 | tf_op jit(solution)/shard_map/all_to_all | solution.py:147
  116.2 0.3 fusion.7
  116.5 0.5 convolution_convert_fusion
  117.0 0.8 copy.115
  117.9 3.5 %all-to-all-start.3 = ((bf16[4,128,2,256]{3,1,2,0:T(8,128)(2,1)}), bf16[4,128,2,256]{3,1,2,0:T(8,128)(2,1)S(1)}, u32[]{:S(2)}, u32[]{:S(2)}) async-start(bf16[4,128,2,256]{3,1,2,0:T(8,128)(2,1)} %bitcast.54), calls=%async_computation.3 | async-start | bytes 1048576 | tf_op jit(solution)/shard_map/all_to_all | solution.py:54
  121.4 0.2 fusion.43
  121.6 0.3 convolution_convert_fusion.2
  121.9 0.6 copy.117
  122.5 8.6 %all-to-all-done.3 = bf16[4,128,2,256]{3,1,2,0:T(8,128)(2,1)S(1)} async-done(((bf16[4,128,2,256]{3,1,2,0:T(8,128)(2,1)}), bf16[4,128,2,256]{3,1,2,0:T(8,128)(2,1)S(1)}, u32[]{:S(2)}, u32[]{:S(2)}) %all-to-all-start.3) | async-done | bytes 524320 | tf_op jit(solution)/shard_map/all_to_all | solution.py:54
  131.1 3.3 %all-to-all-start.5 = ((bf16[4,20,256]{2,1,0:T(8,128)(2,1)}), bf16[4,20,256]{2,1,0:T(8,128)(2,1)S(1)}, u32[]{:S(2)}, u32[]{:S(2)}) async-start(bf16[4,20,256]{2,1,0:T(8,128)(2,1)} %bitcast.56), calls=%async_computation.5 | async-start | bytes 98304 | tf_op jit(solution)/shard_map/all_to_all | solution.py:54
  134.4 0.1 reduce_sum.101
  134.5 0.8 copy.101
  135.3 3.5 %all-to-all-done.5 = bf16[4,20,256]{2,1,0:T(8,128)(2,1)S(1)} async-done(((bf16[4,20,256]{2,1,0:T(8,128)(2,1)}), bf16[4,20,256]{2,1,0:T(8,128)(2,1)S(1)}, u32[]{:S(2)}, u32[]{:S(2)}) %all-to-all-start.5) | async-done | bytes 40992 | tf_op jit(solution)/shard_map/all_to_all | solution.py:54
  138.8 6.9 %all-to-all-start.4 = ((bf16[128,2,256]{2,1,0:T(2,128)(2,1)}), bf16[128,2,256]{2,1,0:T(2,128)(2,1)S(1)}, u32[]{:S(2)}, u32[]{:S(2)}) async-start(bf16[128,2,256]{2,1,0:T(2,128)(2,1)} %copy.101), calls=%async_computation.4 | async-start | bytes 262144 | tf_op jit(solution)/shard_map/all_to_all | solution.py:157
  145.7 12.8 %all-to-all-done.4 = bf16[128,2,256]{2,1,0:T(2,128)(2,1)S(1)} async-done(((bf16[128,2,256]{2,1,0:T(2,128)(2,1)}), bf16[128,2,256]{2,1,0:T(2,128)(2,1)S(1)}, u32[]{:S(2)}, u32[]{:S(2)}) %all-to-all-start.4) | async-done | bytes 131104 | tf_op jit(solution)/shard_map/all_to_all | solution.py:157
  158.6 0.3 fusion.41
  159.0 6.5 %all_to_all.37 = f32[4,1,40]{2,1,0:T(1,128)S(1)} all-to-all(f32[4,1,40]{2,1,0:T(1,128)S(1)} %broadcast_in_dim.20), channel_id=1, replica_groups=mesh['ep'=128,'tp'=4] {'tp'}, dimensions={0} | all-to-all | bytes 1280 | tf_op jit(solution)/shard_map/all_to_all | solution.py:23
  165.5 0.1 slice_multiply_fusion
  165.5 0.7 add_convert_fusion.1
  (51 shorter events, 0.6 us)
Async XLA Ops:
  0.0 116.5 %copy-start = (bf16[1,128,1024]{2,1,0:T(8,128)(2,1)S(1)}, bf16[1,128,1024]{2,1,0:T(8,128)(2,1)}, u32[]{:S(2)}) copy-start(bf16[1,128,1024]{2,1,0:T(8,128)(2,1)} %param.32) | copy-start | bytes 786436
  0.8 1.6 copy-start.8
  0.8 1.7 %copy-start.16 = (f32[8]{0:T(128)S(1)}, f32[8]{0:T(128)}, u32[]{:S(2)}) copy-start(f32[8]{0:T(128)} %param.24) | copy-start | bytes 100
  2.6 52.2 %copy-start.1 = (bf16[5,1024,128]{2,1,0:T(8,128)(2,1)S(1)}, bf16[5,1024,128]{2,1,0:T(8,128)(2,1)}, u32[]{:S(2)}) copy-start(bf16[5,1024,128]{2,1,0:T(8,128)(2,1)} %param.22) | copy-start | bytes 3932164
  55.4 6.2 %copy-start.6 = (s32[20,6]{0,1:T(8,128)S(1)}, s32[20,6]{0,1:T(8,128)}, u32[]{:S(2)}) copy-start(s32[20,6]{0,1:T(8,128)} %param.28) | copy-start | bytes 1444
  55.4 10.5 %copy-start.2 = (bf16[512,256]{1,0:T(8,128)(2,1)S(1)}, bf16[512,256]{1,0:T(8,128)(2,1)}, u32[]{:S(2)}) copy-start(bf16[512,256]{1,0:T(8,128)(2,1)} %param.25) | copy-start | bytes 786436
  55.4 10.5 %copy-start.7 = (bf16[20,256]{1,0:T(8,128)(2,1)S(1)}, bf16[20,256]{1,0:T(8,128)(2,1)}, u32[]{:S(2)}) copy-start(bf16[20,256]{1,0:T(8,128)(2,1)} %param.19) | copy-start | bytes 30724
  55.5 10.7 %copy-start.10 = (f32[256]{0:T(256)S(1)}, f32[256]{0:T(256)}, u32[]{:S(2)}) copy-start(f32[256]{0:T(256)} %param.27) | copy-start | bytes 3076
  55.5 10.7 %copy-start.11 = (f32[256]{0:T(256)S(1)}, f32[256]{0:T(256)}, u32[]{:S(2)}) copy-start(f32[256]{0:T(256)} %param.26) | copy-start | bytes 3076
  55.5 14.6 %copy-start.9 = (f32[20,6]{0,1:T(8,128)S(1)}, f32[20,6]{0,1:T(8,128)}, u32[]{:S(2)}) copy-start(f32[20,6]{0,1:T(8,128)} %param.29) | copy-start | bytes 1444
  56.8 9.1 %all-to-all-start = ((bf16[4,5,512]{2,1,0:T(8,128)(2,1)}), bf16[4,5,512]{2,1,0:T(8,128)(2,1)S(1)}, u32[]{:S(2)}, u32[]{:S(2)}) async-start(bf16[4,5,512]{2,1,0:T(8,128)(2,1)} %broadcast_in_dim.19), calls=%async_computation | async-start | bytes 65536 | tf_op jit(solution)/shard_map/all_to_all | solution.py:23
  66.8 7.9 %all-to-all-start.1 = ((f32[4,256,22]{1,2,0:T(8,128)}), f32[4,256,22]{1,2,0:T(8,128)S(1)}, u32[]{:S(2)}, u32[]{:S(2)}) async-start(f32[4,256,22]{1,2,0:T(8,128)} %stack.2), calls=%async_computation.1 | async-start | bytes 196608 | tf_op jit(solution)/shard_map/all_to_all | solution.py:35
  75.1 41.1 %copy-start.14 = (bf16[1,1024,128]{2,1,0:T(8,128)(2,1)S(1)}, bf16[1,1024,128]{2,1,0:T(8,128)(2,1)}, u32[]{:S(2)}) copy-start(bf16[1,1024,128]{2,1,0:T(8,128)(2,1)} %param.30) | copy-start | bytes 786436
  75.4 41.1 %copy-start.15 = (bf16[1,1024,128]{2,1,0:T(8,128)(2,1)S(1)}, bf16[1,1024,128]{2,1,0:T(8,128)(2,1)}, u32[]{:S(2)}) copy-start(bf16[1,1024,128]{2,1,0:T(8,128)(2,1)} %param.31) | copy-start | bytes 786436
  117.0 4.3 %copy-start.3 = (bf16[1024,128]{1,0:T(8,128)(2,1)S(1)}, bf16[1024,128]{1,0:T(8,128)(2,1)}, u32[]{:S(2)}) copy-start(bf16[1024,128]{1,0:T(8,128)(2,1)} %param.33) | copy-start | bytes 786436
  117.0 4.5 %copy-start.4 = (bf16[128,1024]{1,0:T(8,128)(2,1)S(1)}, bf16[128,1024]{1,0:T(8,128)(2,1)}, u32[]{:S(2)}) copy-start(bf16[128,1024]{1,0:T(8,128)(2,1)} %param.35) | copy-start | bytes 786436
  117.0 4.5 %copy-start.5 = (bf16[1024,128]{1,0:T(8,128)(2,1)S(1)}, bf16[1024,128]{1,0:T(8,128)(2,1)}, u32[]{:S(2)}) copy-start(bf16[1024,128]{1,0:T(8,128)(2,1)} %param.34) | copy-start | bytes 786436
  117.9 13.3 %all-to-all-start.3 = ((bf16[4,128,2,256]{3,1,2,0:T(8,128)(2,1)}), bf16[4,128,2,256]{3,1,2,0:T(8,128)(2,1)S(1)}, u32[]{:S(2)}, u32[]{:S(2)}) async-start(bf16[4,128,2,256]{3,1,2,0:T(8,128)(2,1)} %bitcast.54), calls=%async_computation.3 | async-start | bytes 1048576 | tf_op jit(solution)/shard_map/all_to_all | solution.py:54
  121.5 44.0 %copy-start.12 = (f32[256]{0:T(256)S(1)}, f32[256]{0:T(256)}, u32[]{:S(2)}) copy-start(f32[256]{0:T(256)} %param.37) | copy-start | bytes 3076
  121.5 44.0 %copy-start.13 = (f32[256]{0:T(256)S(1)}, f32[256]{0:T(256)}, u32[]{:S(2)}) copy-start(f32[256]{0:T(256)} %param.36) | copy-start | bytes 3076
  131.1 7.6 %all-to-all-start.5 = ((bf16[4,20,256]{2,1,0:T(8,128)(2,1)}), bf16[4,20,256]{2,1,0:T(8,128)(2,1)S(1)}, u32[]{:S(2)}, u32[]{:S(2)}) async-start(bf16[4,20,256]{2,1,0:T(8,128)(2,1)} %bitcast.56), calls=%async_computation.5 | async-start | bytes 98304 | tf_op jit(solution)/shard_map/all_to_all | solution.py:54
  138.8 19.8 %all-to-all-start.4 = ((bf16[128,2,256]{2,1,0:T(2,128)(2,1)}), bf16[128,2,256]{2,1,0:T(2,128)(2,1)S(1)}, u32[]{:S(2)}, u32[]{:S(2)}) async-start(bf16[128,2,256]{2,1,0:T(2,128)(2,1)} %copy.101), calls=%async_computation.4 | async-start | bytes 262144 | tf_op jit(solution)/shard_map/all_to_all | solution.py:157
